TPU v7x, 32 devices: a whole 2x2x4 slice. The times are simulated.
32 devices in a mesh: sp: 8 (over z, y), tp: 4 (over x, core).
Axes of the slice: x: 2, y: 2, z: 4, core: 2. Of those that a mesh axis runs over, the one named last changes fastest.
Arguments:
- tokens: bfloat16 [2, 4096, 2048], P(None, ('sp', 'tp')), may hold values from -6.5 to 6.5, as said below
- norm_gain: float32 [2048], replicated, may hold values from 0.1 to 1.9
- w_gate: bfloat16 [2048, 4096], P('sp', 'tp'), may hold values from -0.125 to 0.125
- w_value: bfloat16 [2048, 4096], P('sp', 'tp'), may hold values from -0.125 to 0.125
- w_write: bfloat16 [2048, 512], P('sp', 'tp'), may hold values from -0.125 to 0.125
- w_read: bfloat16 [2048, 512], P('sp', 'tp'), may hold values from -0.125 to 0.125
- w_step: bfloat16 [2048, 64], replicated, may hold values from -0.125 to 0.125
- conv_value: float32 [4, 4096], replicated, may hold values from -3 to 3
- conv_write: float32 [4, 512], replicated, may hold values from -3 to 3
- conv_read: float32 [4, 512], replicated, may hold values from -3 to 3
- step_bias: float32 [64], replicated, as said below
- decay_log: float32 [64], replicated, may hold values from 0 to 0.7
- skip_gain: float32 [64], replicated, may hold values from 0.1 to 1.9
- out_gain: float32 [4096], replicated, may hold values from 0.1 to 1.9
- w_out: bfloat16 [4096, 2048], P(None, 'sp'), may hold values from -0.09375 to 0.09375
Outputs:
- mixed: bfloat16 [2, 4096, 2048], P(None, ('sp', 'tp'))
Inputs may be any that keep to these rules, and one draw needn't show every extreme that they name: `tokens`: activations of order one whose mean along a direction drifts slowly over each sequence. `step_bias`: even heads take step offsets between -5.8 and -5.0, odd heads offsets near log(0.12 to 0.33) - log(4096).
All inputs are finite; a program needn't handle non-finite values.
Results may differ from a plain program's by a relative error of at most 0.005.
The roundings to bfloat16 on the way count: a program that leaves them out, or rounds other values in their place, can miss the bound.
Values may be sent and summed in bfloat16 or wider, within the bound.
A program may use at most 192 MiB of HBM per device.

v0:
```python
import jax
import jax.numpy as jnp
from jax import lax
from jax.sharding import PartitionSpec as P

BLOCK = 64
EPSILON = 1e-06
HIGHEST = lax.Precision.HIGHEST


def shifted(x, axis, by):
    devices = lax.axis_size(axis)
    pairs = [(i, i + by) for i in range(devices) if 0 <= i + by < devices]
    return lax.ppermute(x, axis, pairs)


def entering(part, axis, combine, identity):
    place = lax.axis_index(axis)
    gathered = jax.tree.map(lambda a: lax.all_gather(a, axis), part)
    state = jax.tree.map(lambda a, e: jnp.zeros_like(a) + jnp.asarray(e, a.dtype), part, identity)

    def one(step, state):
        return combine(
            state, jax.tree.map(lambda a: lax.dynamic_index_in_dim(a, step, 0, False), gathered)
        )

    return lax.fori_loop(0, place, one, state)


def rms_scale(values, gain_vec):
    return (
        values * lax.rsqrt(jnp.mean(values * values, axis=-1, keepdims=True) + EPSILON) * gain_vec
    )


def convolve(local_rows, earlier, kernel):
    tap_count = kernel.shape[0]
    length = local_rows.shape[1]
    padded = jnp.concatenate([earlier, local_rows], axis=1).astype(jnp.float32)
    running = padded[:, 0:length, :] * kernel[0]
    for offset in range(1, tap_count):
        running = running + padded[:, offset : offset + length, :] * kernel[offset]
    return jax.nn.silu(running)


def merge_states(earlier, later):
    return (earlier[0] * later[0], earlier[1] * later[0][:, :, None, None] + later[1])


def body(
    tokens,
    norm_gain,
    w_gate,
    w_value,
    w_write,
    w_read,
    w_step,
    conv_value,
    conv_write,
    conv_read,
    step_bias,
    decay_log,
    skip_gain,
    out_gain,
    w_out,
):
    seq_count, own_rows, model_width = tokens.shape
    group_devs = lax.axis_size("tp")
    tp_rank = lax.axis_index("tp")
    head_count = w_step.shape[1]
    local_heads = head_count // group_devs
    channels = w_gate.shape[1]
    head_dim = channels // local_heads
    state_dim = w_write.shape[1]
    tap_count = conv_value.shape[0]
    group_rows = own_rows * group_devs
    normed = rms_scale(tokens.astype(jnp.float32), norm_gain).astype(jnp.bfloat16)
    whole_gate, whole_value, whole_write, whole_read, whole_out = (
        lax.all_gather(w_gate, "sp", axis=0, tiled=True),
        lax.all_gather(w_value, "sp", axis=0, tiled=True),
        lax.all_gather(w_write, "sp", axis=0, tiled=True),
        lax.all_gather(w_read, "sp", axis=0, tiled=True),
        lax.all_gather(w_out, "sp", axis=1, tiled=True),
    )
    first_head = tp_rank * local_heads
    step_cols = lax.dynamic_slice_in_dim(w_step, first_head, local_heads, 1)
    projections = (whole_gate, whole_value, whole_write, whole_read)

    def empty_rows(cols, dtype):
        return jnp.zeros((seq_count, group_rows, cols), dtype)

    initial = (
        empty_rows(channels, jnp.bfloat16),
        empty_rows(channels, jnp.bfloat16),
        empty_rows(state_dim, jnp.bfloat16),
        empty_rows(state_dim, jnp.bfloat16),
        empty_rows(local_heads, jnp.float32),
    )
    shard_piece = lax.all_gather(normed, "tp", axis=1, tiled=True)
    piece_rows = shard_piece.shape[1]
    flat_piece = shard_piece.reshape(seq_count * piece_rows, model_width)
    updated = []
    for target, weight in zip(initial[:4], projections):
        projected = jnp.dot(flat_piece, weight, preferred_element_type=jnp.float32)
        projected = projected.astype(jnp.bfloat16).reshape(seq_count, piece_rows, weight.shape[1])
        updated.append(projected)
    step_piece = jnp.dot(flat_piece, step_cols, preferred_element_type=jnp.float32)
    step_piece = step_piece.reshape(seq_count, piece_rows, local_heads)
    updated.append(step_piece)
    gate_in, value_in, write_in, read_in, step_raw = tuple(updated)
    keep_from = group_rows - tap_count + 1
    tail_rows = jnp.concatenate(
        [value_in[:, keep_from:], write_in[:, keep_from:], read_in[:, keep_from:]], axis=2
    )
    before = shifted(tail_rows, "sp", 1)
    kernel_value = lax.dynamic_slice_in_dim(conv_value, first_head * head_dim, channels, 1)
    kernel_write = lax.dynamic_slice_in_dim(conv_write, tp_rank * state_dim, state_dim, 1)
    kernel_read = lax.dynamic_slice_in_dim(conv_read, tp_rank * state_dim, state_dim, 1)
    value_conv = convolve(value_in, before[:, :, :channels], kernel_value)
    write_conv = convolve(write_in, before[:, :, channels : channels + state_dim], kernel_write)
    read_conv = convolve(read_in, before[:, :, channels + state_dim :], kernel_read)
    step_size = jax.nn.softplus(
        step_raw + lax.dynamic_slice_in_dim(step_bias, first_head, local_heads, 0)
    )
    decay_rate = -jnp.exp(lax.dynamic_slice_in_dim(decay_log, first_head, local_heads, 0))
    skip_local = lax.dynamic_slice_in_dim(skip_gain, first_head, local_heads, 0)
    block_count = group_rows // BLOCK
    value_blocks = value_conv.reshape(seq_count, block_count, BLOCK, local_heads, head_dim)
    step_blocks = jnp.moveaxis(step_size.reshape(seq_count, block_count, BLOCK, local_heads), 3, 2)
    write_blocks = write_conv.reshape(seq_count, block_count, BLOCK, state_dim)
    read_blocks = read_conv.reshape(seq_count, block_count, BLOCK, state_dim)
    log_decay = jnp.cumsum(step_blocks * decay_rate[:, None], axis=3)
    value_steps = value_blocks * jnp.moveaxis(step_blocks, 3, 2)[..., None]
    causal_mask = jnp.arange(BLOCK)[:, None] >= jnp.arange(BLOCK)[None, :]
    log_gap = log_decay[..., :, None] - log_decay[..., None, :]
    weights = jnp.exp(jnp.where(causal_mask, log_gap, -jnp.inf))
    intersect = jnp.einsum("skln,skmn->sklm", read_blocks, write_blocks, precision=HIGHEST)
    scores = weights * intersect[:, :, None]
    inner = jnp.einsum("skhlm,skmhp->sklhp", scores, value_steps, precision=HIGHEST)
    block_decay = log_decay[..., -1]
    fade_out = jnp.exp(block_decay[..., None] - log_decay)
    states = jnp.einsum(
        "skmn,skhm,skmhp->skhpn", write_blocks, fade_out, value_steps, precision=HIGHEST
    )
    run_sum = jnp.cumsum(block_decay, axis=1)
    run_before = run_sum - block_decay
    block_ids = jnp.arange(block_count)
    later_mask = (block_ids[:, None] > block_ids[None, :])[:, :, None]
    between = jnp.exp(
        jnp.where(later_mask, run_before[:, :, None, :] - run_sum[:, None, :, :], -jnp.inf)
    )
    prev_state = jnp.einsum("skjh,sjhpn->skhpn", between, states, precision=HIGHEST)
    total_fade = jnp.exp(run_sum[:, -1:, :] - run_sum)
    dev_state = jnp.einsum("sjh,sjhpn->shpn", total_fade, states, precision=HIGHEST)
    dev_decay = jnp.exp(run_sum[:, -1, :])
    identity = (jnp.ones_like(dev_decay), jnp.zeros_like(dev_state))
    incoming = entering((dev_decay, dev_state), "sp", merge_states, identity)[1]
    read_scale = jnp.exp(log_decay)
    local_part = jnp.einsum(
        "skln,skhpn,skhl->sklhp", read_blocks, prev_state, read_scale, precision=HIGHEST
    )
    outer_part = jnp.einsum(
        "skln,shpn,skhl->sklhp",
        read_blocks,
        incoming,
        jnp.exp(run_before[..., None] + log_decay),
        precision=HIGHEST,
    )
    carried = local_part + outer_part
    heads_out = (inner + carried + skip_local[:, None] * value_blocks).reshape(
        seq_count, group_rows, channels
    )
    gated = (heads_out * jax.nn.silu(gate_in.astype(jnp.float32))).astype(jnp.bfloat16)
    token_rows = lax.all_to_all(gated, "tp", split_axis=1, concat_axis=2, tiled=True)
    mixed_in = rms_scale(token_rows.astype(jnp.float32), out_gain).astype(jnp.bfloat16)
    flat_mixed = mixed_in.reshape(seq_count * own_rows, mixed_in.shape[2])
    result = jnp.dot(flat_mixed, whole_out, preferred_element_type=jnp.float32).astype(jnp.bfloat16)
    return result.reshape(seq_count, own_rows, model_width)


def solution(mesh):
    in_specs = (
        P(None, ("sp", "tp"), None),
        P(),
        P("sp", "tp"),
        P("sp", "tp"),
        P("sp", "tp"),
        P("sp", "tp"),
        P(),
        P(),
        P(),
        P(),
        P(),
        P(),
        P(),
        P(),
        P(None, "sp"),
    )
    out_specs = P(None, ("sp", "tp"), None)
    return jax.shard_map(body, mesh=mesh, in_specs=in_specs, out_specs=out_specs, check_vma=False)
```

profile of v0, /device:TPU:0, one launch (start us, length us, event | category | flops | bytes accessed | tf_op | source)
XLA Modules:
  0.0 570.5 jit_solution(64083504945850999)
XLA Ops:
  8.2 2.5 fusion.35
  12.4 33.1 %all_gather.30 = bf16[2048,128]{1,0:T(8,128)(2,1)S(1)} all-gather(bf16[256,128]{1,0:T(8,128)(2,1)S(1)} %copy-done.10), channel_id=1, replica_groups=mesh['sp'=8,'tp'=4] {'sp'}, dimensions={0}, use_global_device_ids=true | all-gather | bytes 589824 | tf_op jit(solution)/shard_map/all_gather | solution.py:81
  45.5 32.9 %all_gather.31 = bf16[2048,128]{1,0:T(8,128)(2,1)S(1)} all-gather(bf16[256,128]{1,0:T(8,128)(2,1)S(1)} %copy-done.11), channel_id=1, replica_groups=mesh['sp'=8,'tp'=4] {'sp'}, dimensions={0}, use_global_device_ids=true | all-gather | bytes 589824 | tf_op jit(solution)/shard_map/all_gather | solution.py:82
  81.9 3.4 compare_select_fusion
  85.4 3.5 reduce_window_sum.24
  89.4 3.6 convolution_convert_fusion.4
  96.0 28.8 %all-gather.10.cloned.1.call-done = bf16[2048,1024]{1,0:T(8,128)(2,1)} async-done(((bf16[256,1024]{1,0:T(8,128)(2,1)}), bf16[2048,1024]{1,0:T(8,128)(2,1)}) %all-gather.10.cloned.1.call-update) | async-done | bytes 4194320 | tf_op jit(solution)/shard_map/all_gather | solution.py:80
  124.8 7.9 %convolution_convert_fusion.2 = bf16[1024,1024]{1,0:T(8,128)(2,1)S(1)} fusion(bf16[1024,2048]{1,0:T(8,128)(2,1)} %bitcast.120, bf16[2048,1024]{1,0:T(8,128)(2,1)} %all-gather.10.cloned.1.call-done), kind=kOutput, calls=%fused_computation.53 | convolution fusion | flops 4296015872 | bytes 10485760 | tf_op jit(solution)/shard_map/dot_general | solution.py:104
  133.4 3.1 collective-permute-start
  140.5 4.6 divide_multiply_fusion
  145.1 7.4 %reshape.114 = f32[2,8,64,16,64]{4,3,2,1,0:T(8,128)} reshape(f32[2,512,1024]{2,1,0:T(8,128)} %divide_multiply_fusion) | data formatting | bytes 8388608 | tf_op jit(solution)/shard_map/reshape | solution.py:128
  153.7 9.0 %broadcast_multiply_fusion = (f32[2,8,64,16,64]{4,3,2,1,0:T(8,128)S(1)}, f32[2,8,64,16,64]{4,3,2,1,0:T(8,128)}) fusion(f32[2,8,64,16]{3,2,1,0:T(8,128)S(1)} %copy.101, f32[2,8,64,16,64]{4,3,2,1,0:T(8,128)} %reshape.114, f32[2,8,64,16]{3,2,1,0:T(8,128)S(1)} %copy.98), kind=kLoop, calls=%fused_computation.33 | loop fusion | flops 2097152 | bytes 12713984 | tf_op jit(solution)/shard_map/skmn,skhm,skmhp->skhpn/dot_general | solution.py:142
  162.7 15.2 %fusion.3 = f32[2,8,16,64,128]{4,3,2,1,0:T(8,128)S(1)} fusion(f32[2,8,64,128,1]{3,2,4,1,0:T(8,128)S(1)} %bitcast.117, f32[2,8,64,16,64]{4,3,2,1,0:T(8,128)S(1)} %get-tuple-element.60), kind=kOutput, calls=%fused_computation.6 | convolution fusion | flops 1610612736 | bytes 13107200 | tf_op jit(solution)/shard_map/skmn,skhm,skmhp->skhpn/dot_general | solution.py:142
  177.9 11.7 %fusion.11 = f32[2,16,1,64,128]{4,2,3,1,0:T(1,128)} fusion(f32[2,8,16,1,1]{1,3,4,2,0:T(1,128)S(1)} %copy.119, f32[2,8,16,64,128]{4,3,2,1,0:T(8,128)S(1)} %fusion.3), kind=kOutput, calls=%fused_computation.14 | convolution fusion | flops 25165824 | bytes 9438208 | tf_op jit(solution)/shard_map/sjh,sjhpn->shpn/dot_general | solution.py:154
  190.5 18.6 %all-gather = f32[16,1,16]{2,1,0:T(1,128)S(1)} all-gather(f32[2,1,16]{2,1,0:T(1,128)S(1)} %copy-done.13), channel_id=2, replica_groups=mesh['sp'=8,'tp'=4] {'sp'}, dimensions={0}, use_global_device_ids=true | all-gather | bytes 1152 | tf_op jit(solution)/shard_map/all_gather | solution.py:19
  209.1 9.4 %convolution_convert_fusion.1 = bf16[1024,1024]{1,0:T(8,128)(2,1)} fusion(bf16[1024,2048]{1,0:T(8,128)(2,1)} %bitcast.121, bf16[2048,1024]{1,0:T(8,128)(2,1)} %all-gather.12.cloned.1.call-done), kind=kOutput, calls=%fused_computation.52 | convolution fusion | flops 4296015872 | bytes 10485760 | tf_op jit(solution)/shard_map/dot_general | solution.py:104
  218.4 9.2 %copy.110 = f32[2,8,64,16,64]{2,4,3,1,0:T(8,128)} copy(f32[2,8,64,16,64]{4,3,2,1,0:T(8,128)} %reshape.114) | data formatting | bytes 8388608 | tf_op jit(solution)/shard_map/reshape | solution.py:128
  228.9 17.3 %fusion.30 = f32[2,8,16,64,128]{4,1,3,2,0:T(8,128)} fusion(f32[2,8,16,64,128]{4,3,2,1,0:T(8,128)} %copy-done.2, f32[2,8,16]{1,2,0:T(8,128)S(1)} %copy.104, f32[2,8,16]{1,2,0:T(8,128)S(1)} %copy.103, pred[8,8]{1,0:T(8,128)(4,1)S(1)} %iota_compare_fusion.1), kind=kOutput, calls=%fused_computation.42 | convolution fusion | flops 201330688 | bytes 16779328 | tf_op jit(solution)/shard_map/skjh,sjhpn->skhpn/dot_general | solution.py:152
  246.2 17.5 %fusion.5 = f32[2,8,16,64,64]{4,3,2,1,0:T(8,128)} fusion(f32[2,8,64,16,64]{4,3,2,1,0:T(8,128)S(1)} %bitcast.111, f32[2,8,64,64]{3,2,1,0:T(8,128)S(1)} %fusion.65, f32[2,8,16,64]{3,2,1,0:T(8,128)S(1)} %reduce_window_sum.24, pred[64,64]{1,0:T(8,128)(4,1)S(1)} %iota_compare_fusion), kind=kOutput, calls=%fused_computation.8 | convolution fusion | flops 808452096 | bytes 8720384 | tf_op jit(solution)/shard_map/skhlm,skmhp->sklhp/dot_general | solution.py:139
  263.8 60.0 %all-gather.16.cloned.1.call-done = f32[16,16,64,128]{3,2,1,0:T(8,128)} async-done(((f32[2,16,64,128]{3,2,1,0:T(8,128)}), f32[16,16,64,128]{3,2,1,0:T(8,128)}) %all-gather.16.cloned.1.call-update) | async-done | bytes 8388624 | tf_op jit(solution)/shard_map/all_gather | solution.py:19
  323.9 9.5 %fusion.38 = f32[2,8,64,16,64]{2,4,3,1,0:T(8,128)} fusion(f32[2,8,64,128,1]{3,2,4,1,0:T(8,128)S(1)} %bitcast.115, f32[2,16,64,128]{3,2,1,0:T(8,128)S(1)} %get-tuple-element.49), kind=kOutput, calls=%fused_computation.57 | convolution fusion | flops 1610612736 | bytes 5767168 | tf_op jit(solution)/shard_map/skln,shpn,skhl->sklhp/dot_general | solution.py:162
  333.4 19.5 %fusion = f32[2,8,64,16,64]{2,4,3,1,0:T(8,128)} fusion(f32[2,8,16,64,64]{4,3,2,1,0:T(8,128)} %fusion.5, f32[2,8,64,16,64]{2,4,3,1,0:T(8,128)} %copy.110, f32[2,8,64,16,64]{2,4,3,1,0:T(8,128)} %fusion.38, f32[16]{0:T(128)S(1)} %dynamic_slice.37, f32[2,8,64,16]{2,3,1,0:T(8,128)S(1)} %copy-done.5, f32[2,8,64,16]{2,3,1,0:T(8,128)S(1)} %get-tuple-element.62, ...), kind=kOutput, calls=%fused_computation.3 | convolution fusion | flops 1616904192 | bytes 25821248 | tf_op jit(solution)/shard_map/skln,skhpn,skhl->sklhp/dot_general | solution.py:159
  352.9 9.2 %copy.111 = f32[2,8,64,16,64]{4,3,2,1,0:T(8,128)} copy(f32[2,8,64,16,64]{2,4,3,1,0:T(8,128)} %fusion) | data formatting | bytes 8388608 | tf_op jit(solution)/shard_map/add | solution.py:170
  362.1 8.0 %reshape.117 = f32[2,512,1024]{2,1,0:T(8,128)} reshape(f32[2,8,64,16,64]{4,3,2,1,0:T(8,128)} %copy.111) | data formatting | bytes 8388608 | tf_op jit(solution)/shard_map/reshape | solution.py:170
  370.1 3.5 fusion.26
  373.6 2.2 copy.112
  375.8 28.3 %all_to_all.4 = bf16[2,512,1024]{2,0,1:T(2,128)(2,1)S(1)} all-to-all(bf16[2,512,1024]{2,0,1:T(2,128)(2,1)S(1)} %copy.112), channel_id=1, replica_groups=mesh['sp'=8,'tp'=4] {'tp'}, dimensions={1} | all-to-all | bytes 4194304 | tf_op jit(solution)/shard_map/all_to_all | solution.py:174
  404.1 1.6 copy.113
  405.7 5.8 %copy.123 = f32[32,8,4,1024]{3,1,2,0:T(8,128)} copy(f32[32,8,4,1024]{3,2,1,0:T(4,128)S(1)} %bitcast.113) | data formatting | bytes 8388608
  411.5 2.2 multiply_reduce_fusion
  413.9 137.3 %all-gather.14.cloned.1.call-done = bf16[4096,2048]{1,0:T(8,128)(2,1)} async-done(((bf16[4096,256]{1,0:T(8,128)(2,1)}), bf16[4096,2048]{1,0:T(8,128)(2,1)}) %all-gather.14.cloned.1.call-update) | async-done | bytes 16777232 | tf_op jit(solution)/shard_map/all_gather | solution.py:83
  551.2 12.6 %convolution_convert_fusion = bf16[256,2048]{1,0:T(8,128)(2,1)} fusion(bf16[4096,2048]{1,0:T(8,128)(2,1)} %all-gather.14.cloned.1.call-done, f32[256,4096]{1,0:T(8,128)} %bitcast.124, f32[4096]{0:T(1024)S(1)} %copy-done.18, f32[256]{0:T(256)S(1)} %bitcast.141), kind=kOutput, calls=%fused_computation.45 | convolution fusion | flops 4298637312 | bytes 22037504 | tf_op jit(solution)/shard_map/dot_general | solution.py:177
  (104 shorter events, 18.4 us)
Async XLA Ops:
  6.5 75.3 %copy-start = (bf16[2048,64]{0,1:T(8,128)(2,1)S(1)}, bf16[2048,64]{0,1:T(8,128)(2,1)}, u32[]{:S(2)}) copy-start(bf16[2048,64]{0,1:T(8,128)(2,1)} %param.23) | copy-start | bytes 786436
  6.5 5.7 %copy-start.19 = (f32[64]{0:T(128)S(1)}, f32[64]{0:T(128)}, u32[]{:S(2)}) copy-start(f32[64]{0:T(128)} %param.27) | copy-start | bytes 772
  6.5 5.8 %copy-start.20 = (f32[64]{0:T(128)S(1)}, f32[64]{0:T(128)}, u32[]{:S(2)}) copy-start(f32[64]{0:T(128)} %param.28) | copy-start | bytes 772
  6.5 5.9 %copy-start.10 = (bf16[256,128]{1,0:T(8,128)(2,1)S(1)}, bf16[256,128]{1,0:T(8,128)(2,1)}, u32[]{:S(2)}) copy-start(bf16[256,128]{1,0:T(8,128)(2,1)} %param.21) | copy-start | bytes 196612
  6.5 39.0 %copy-start.11 = (bf16[256,128]{1,0:T(8,128)(2,1)S(1)}, bf16[256,128]{1,0:T(8,128)(2,1)}, u32[]{:S(2)}) copy-start(bf16[256,128]{1,0:T(8,128)(2,1)} %param.22) | copy-start | bytes 196612
  6.5 75.3 %all-gather.8.cloned.1.call-start = ((), (), s32[]{:S(2)}) async-start(), calls=%async_computation.1 | async-start | bytes 5242880 | tf_op jit(solution)/shard_map/all_gather | solution.py:99
  10.7 114.0 %all-gather.10.cloned.1.call-start = ((), (), s32[]{:S(2)}) async-start(), calls=%async_computation.2 | async-start | bytes 4718592 | tf_op jit(solution)/shard_map/all_gather | solution.py:80
  11.5 197.6 %all-gather.12.cloned.1.call-start = ((), (), s32[]{:S(2)}) async-start(), calls=%async_computation.3 | async-start | bytes 4718592 | tf_op jit(solution)/shard_map/all_gather | solution.py:79
  12.2 311.5 %all-gather.16.cloned.1.call-start = ((), (), s32[]{:S(2)}) async-start(), calls=%async_computation.5 | async-start | bytes 9437184 | tf_op jit(solution)/shard_map/all_gather | solution.py:19
  89.4 3.6 copy-start.3
  93.0 1.5 copy-start.6
  94.3 1.7 copy-start.8
  133.4 5.8 %collective-permute-start = (bf16[2,3,1280]{2,1,0:T(4,128)(2,1)}, bf16[2,3,1280]{2,1,0:T(4,128)(2,1)}, u32[]{:S(2)}, u32[]{:S(2)}) collective-permute-start(bf16[2,3,1280]{2,1,0:T(4,128)(2,1)} %pad_maximum_fusion), channel_id=1, source_target_pairs={{0,4},{4,8},{8,12},{12,16},{16,20},{20,24},{24,28},{1,5},{5,9},{9,... | collective-permute-start | bytes 46088 | tf_op jit(solution)/shard_map/ppermute | solution.py:14
  145.1 8.1 %copy-start.7 = (bf16[1024,128]{1,0:T(8,128)(2,1)S(1)}, bf16[1024,128]{1,0:T(8,128)(2,1)}, u32[]{:S(2)}) copy-start(bf16[1024,128]{1,0:T(8,128)(2,1)} %copy-done.6) | copy-start | bytes 786436
  145.1 8.1 %copy-start.9 = (bf16[1024,128]{1,0:T(8,128)(2,1)S(1)}, bf16[1024,128]{1,0:T(8,128)(2,1)}, u32[]{:S(2)}) copy-start(bf16[1024,128]{1,0:T(8,128)(2,1)} %copy-done.8) | copy-start | bytes 786436
  145.1 8.2 %copy-start.14 = (f32[128]{0:T(128)S(1)}, f32[128]{0:T(128)}, u32[]{:S(2)}) copy-start(f32[128]{0:T(128)} %get-tuple-element.75) | copy-start | bytes 1540
  145.1 8.2 %copy-start.15 = (f32[128]{0:T(128)S(1)}, f32[128]{0:T(128)}, u32[]{:S(2)}) copy-start(f32[128]{0:T(128)} %get-tuple-element.76) | copy-start | bytes 1540
  145.1 8.2 %copy-start.16 = (f32[128]{0:T(128)S(1)}, f32[128]{0:T(128)}, u32[]{:S(2)}) copy-start(f32[128]{0:T(128)} %get-tuple-element.77) | copy-start | bytes 1540
  145.1 8.2 %copy-start.17 = (f32[128]{0:T(128)S(1)}, f32[128]{0:T(128)}, u32[]{:S(2)}) copy-start(f32[128]{0:T(128)} %get-tuple-element.78) | copy-start | bytes 1540
  177.8 11.7 %copy-start.2 = (f32[2,8,16,64,128]{4,3,2,1,0:T(8,128)}, f32[2,8,16,64,128]{4,3,2,1,0:T(8,128)S(1)}, u32[]{:S(2)}) copy-start(f32[2,8,16,64,128]{4,3,2,1,0:T(8,128)S(1)} %fusion.3) | copy-start | bytes 25165828
  177.9 12.3 %copy-start.21 = (f32[64]{0:T(128)S(1)}, f32[64]{0:T(128)}, u32[]{:S(2)}) copy-start(f32[64]{0:T(128)} %param.29) | copy-start | bytes 772
  177.9 12.4 %copy-start.12 = (f32[4,128]{1,0:T(4,128)S(1)}, f32[4,128]{1,0:T(4,128)}, u32[]{:S(2)}) copy-start(f32[4,128]{1,0:T(4,128)} %get-tuple-element.86) | copy-start | bytes 6148
  177.9 12.6 %copy-start.13 = (f32[2,1,16]{2,1,0:T(1,128)S(1)}, f32[2,1,16]{2,1,0:T(1,128)}, u32[]{:S(2)}) copy-start(f32[2,1,16]{2,1,0:T(1,128)} %get-tuple-element.74) | copy-start | bytes 388
  189.6 361.6 %all-gather.14.cloned.1.call-start = ((), (), s32[]{:S(2)}) async-start(), calls=%async_computation.4 | async-start | bytes 18874368 | tf_op jit(solution)/shard_map/all_gather | solution.py:83
  227.9 18.3 %slice-start = ((s8[8388608]{0:T(1024)(128)(4,1)}), s8[4194304]{0:T(1024)(128)(4,1)S(1)}, s32[]{:S(2)}) async-start(s8[8388608]{0:T(1024)(128)(4,1)} %bitcast.110), calls=%async_computation.6 | async-start | bytes 8388608
  228.9 17.3 %slice-start.1 = ((s8[8388608]{0:T(1024)(128)(4,1)}), s8[4194304]{0:T(1024)(128)(4,1)S(1)}, s32[]{:S(2)}) async-start(s8[8388608]{0:T(1024)(128)(4,1)} %bitcast.110), calls=%async_computation.7 | async-start | bytes 8388608
  323.9 9.5 %copy-start.5 = (f32[2,8,64,16]{2,3,1,0:T(8,128)S(1)}, f32[2,8,64,16]{2,3,1,0:T(8,128)}, u32[]{:S(2)}) copy-start(f32[2,8,64,16]{2,3,1,0:T(8,128)} %get-tuple-element.64) | copy-start | bytes 196612
  362.1 8.0 %copy-start.4 = (bf16[1024,1024]{1,0:T(8,128)(2,1)S(1)}, bf16[1024,1024]{1,0:T(8,128)(2,1)}, u32[]{:S(2)}) copy-start(bf16[1024,1024]{1,0:T(8,128)(2,1)} %convolution_convert_fusion.1) | copy-start | bytes 6291460
  405.7 145.4 %copy-start.18 = (f32[4096]{0:T(1024)S(1)}, f32[4096]{0:T(1024)}, u32[]{:S(2)}) copy-start(f32[4096]{0:T(1024)} %param.30) | copy-start | bytes 49156
  551.2 12.6 %copy-start.1 = (bf16[2048,64]{0,1:T(8,128)(2,1)S(1)}, bf16[2048,64]{0,1:T(8,128)(2,1)}, u32[]{:S(2)}) copy-start(bf16[2048,64]{0,1:T(8,128)(2,1)} %param.23) | copy-start | bytes 786436
Sparse Core Ops, SparseCore 0:
  10.8 37.1 all-gather.7
  50.2 74.5 all-gather.9
  126.9 71.7 all-gather.11
  200.7 123.0 all-gather.15
  325.6 225.4 all-gather.13
where the time goes:
time: 580 us; the launch traced here: 570 us
  waiting for transfers between devices  228 us (39%)
  matrix products  130 us (22%)
  blocking collectives  113 us (19%)
  local copies, waits for them, and re-layouts  51.9 us (9%)
  other arithmetic  30.8 us (5%)
  between operations  13.8 us (2%)
    all_gather x1, waiting for transfers between devices, body(): lax.all_gather(w_out, 'sp', axis=1, tiled=True)  137 us
    all_gather x1, waiting for transfers between devices, entering(): gathered = jax.tree.map(lambda a: lax.all_gather(a, axis), part)  60 us
    all_gather x1, blocking collectives, body(): lax.all_gather(w_write, 'sp', axis=0, tiled=True)  33.1 us
    all_gather x1, blocking collectives, body(): lax.all_gather(w_read, 'sp', axis=0, tiled=True)  32.9 us
    all_gather x1, waiting for transfers between devices, body(): lax.all_gather(w_value, 'sp', axis=0, tiled=True)  28.8 us
    all_to_all x1, blocking collectives, body(): lax.all_to_all(gated, 'tp', split_axis=1, concat_axis=2, tiled=True)  28.3 us
    dot_general x4, matrix products, body(): projected = jnp.dot(flat_piece, weight, preferred_element_type=jnp.float32)  22.1 us
    dot_general x1, matrix products, body(): jnp.einsum('skln,skhpn,skhl->sklhp', read_blocks, prev_state, read_scale,...  19.5 us
  transfers between devices with their start and end apart: 6, of which 3 were waited for; matrix products, arithmetic and copies ran while one was open for 34% of the time, Pallas kernels for 0%

commit v1 on v0

--- a/solution.py
+++ b/solution.py
@@ -6,6 +6,16 @@
 BLOCK = 64
 EPSILON = 1e-06
 HIGHEST = lax.Precision.HIGHEST
+
+
+def collect(x, axis, dim):
+    ways, here, hop = (lax.axis_size(axis), lax.axis_index(axis), x.shape[dim])
+    shape = [n * ways if d == dim else n for d, n in enumerate(x.shape)]
+    full = lax.dynamic_update_slice_in_dim(jnp.zeros(shape, x.dtype), x, here * hop, axis=dim)
+    for far in range(1, ways):
+        x = lax.ppermute(x, axis, [(d, (d + 1) % ways) for d in range(ways)])
+        full = lax.dynamic_update_slice_in_dim(full, x, (here - far) % ways * hop, axis=dim)
+    return full
 
 
 def shifted(x, axis, by):
@@ -80,7 +90,7 @@
         lax.all_gather(w_value, "sp", axis=0, tiled=True),
         lax.all_gather(w_write, "sp", axis=0, tiled=True),
         lax.all_gather(w_read, "sp", axis=0, tiled=True),
-        lax.all_gather(w_out, "sp", axis=1, tiled=True),
+        collect(w_out, "sp", 1),
     )
     first_head = tp_rank * local_heads
     step_cols = lax.dynamic_slice_in_dim(w_step, first_head, local_heads, 1)

time: 580 us -> 730 us (1.26)
  the two profiles are of different devices: /device:TPU:0 before, /device:TPU:28 now
where the time goes in v1:
time: 730 us; the launch traced here: 720 us
  waiting for transfers between devices  323 us (44%)
  matrix products  129 us (18%)
  blocking collectives  105 us (14%)
  local copies, waits for them, and re-layouts  82.7 us (11%)
  other arithmetic  40.7 us (6%)
  starting transfers between devices  26 us (4%)
  between operations  13.9 us (2%)
    ppermute x7, waiting for transfers between devices, collect(): x = lax.ppermute(x, axis, [(d, (d + 1) % ways) for d in range(ways)])  280 us
    all_gather x1, blocking collectives, entering(): gathered = jax.tree.map(lambda a: lax.all_gather(a, axis), part)  40.7 us
    all_gather x1, blocking collectives, body(): lax.all_gather(w_read, 'sp', axis=0, tiled=True)  33.2 us
    all_gather x1, blocking collectives, body(): lax.all_gather(w_write, 'sp', axis=0, tiled=True)  31.5 us
    all_gather x1, waiting for transfers between devices, body(): lax.all_gather(w_value, 'sp', axis=0, tiled=True)  25.8 us
    dot_general x4, matrix products, body(): projected = jnp.dot(flat_piece, weight, preferred_element_type=jnp.float32)  22.1 us
    ppermute x7, starting transfers between devices, collect(): x = lax.ppermute(x, axis, [(d, (d + 1) % ways) for d in range(ways)])  21 us
    dot_general x1, matrix products, body(): jnp.einsum('skln,skhpn,skhl->sklhp', read_blocks, prev_state, read_scale,...  18.8 us
  transfers between devices with their start and end apart: 13, of which 7 were waited for; matrix products, arithmetic and copies ran while one was open for 31% of the time, Pallas kernels for 0%

profile of v1, /device:TPU:28, one launch (start us, length us, event | category | flops | bytes accessed | tf_op | source)
XLA Modules:
  0.0 720.3 jit_solution(17187487857526046789)
XLA Ops:
  12.4 31.5 %all_gather.27 = bf16[2048,128]{1,0:T(8,128)(2,1)S(1)} all-gather(bf16[256,128]{1,0:T(8,128)(2,1)S(1)} %copy-done.15), channel_id=1, replica_groups=mesh['sp'=8,'tp'=4] {'sp'}, dimensions={0}, use_global_device_ids=true | all-gather | bytes 589824 | tf_op jit(solution)/shard_map/all_gather | solution.py:91
  43.9 33.2 %all_gather.28 = bf16[2048,128]{1,0:T(8,128)(2,1)S(1)} all-gather(bf16[256,128]{1,0:T(8,128)(2,1)S(1)} %copy-done.16), channel_id=1, replica_groups=mesh['sp'=8,'tp'=4] {'sp'}, dimensions={0}, use_global_device_ids=true | all-gather | bytes 589824 | tf_op jit(solution)/shard_map/all_gather | solution.py:92
  88.2 3.6 convolution_convert_fusion.4
  94.7 25.8 %all-gather.9.cloned.1.call-done = bf16[2048,1024]{1,0:T(8,128)(2,1)} async-done(((bf16[256,1024]{1,0:T(8,128)(2,1)}), bf16[2048,1024]{1,0:T(8,128)(2,1)}) %all-gather.9.cloned.1.call-update) | async-done | bytes 4194320 | tf_op jit(solution)/shard_map/all_gather | solution.py:90
  120.6 7.9 %convolution_convert_fusion.2 = bf16[1024,1024]{1,0:T(8,128)(2,1)S(1)} fusion(bf16[1024,2048]{1,0:T(8,128)(2,1)} %bitcast.120, bf16[2048,1024]{1,0:T(8,128)(2,1)} %all-gather.9.cloned.1.call-done), kind=kOutput, calls=%fused_computation.53 | convolution fusion | flops 4296015872 | bytes 10485760 | tf_op jit(solution)/shard_map/dot_general | solution.py:114
  136.9 4.6 divide_multiply_fusion
  141.5 7.4 %reshape.114 = f32[2,8,64,16,64]{4,3,2,1,0:T(8,128)} reshape(f32[2,512,1024]{2,1,0:T(8,128)} %divide_multiply_fusion) | data formatting | bytes 8388608 | tf_op jit(solution)/shard_map/reshape | solution.py:138
  150.1 8.7 %broadcast_multiply_fusion = (f32[2,8,64,16,64]{4,3,2,1,0:T(8,128)S(1)}, f32[2,8,64,16,64]{4,3,2,1,0:T(8,128)}) fusion(f32[2,8,64,16]{3,2,1,0:T(8,128)S(1)} %copy.101, f32[2,8,64,16,64]{4,3,2,1,0:T(8,128)} %reshape.114, f32[2,8,64,16]{3,2,1,0:T(8,128)S(1)} %copy.98), kind=kLoop, calls=%fused_computation.33 | loop fusion | flops 2097152 | bytes 12713984 | tf_op jit(solution)/shard_map/skmn,skhm,skmhp->skhpn/dot_general | solution.py:152
  158.8 15.0 %fusion.3 = f32[2,8,16,64,128]{4,3,2,1,0:T(8,128)S(1)} fusion(f32[2,8,64,128,1]{3,2,4,1,0:T(8,128)S(1)} %bitcast.117, f32[2,8,64,16,64]{4,3,2,1,0:T(8,128)S(1)} %get-tuple-element.60), kind=kOutput, calls=%fused_computation.6 | convolution fusion | flops 1610612736 | bytes 13107200 | tf_op jit(solution)/shard_map/skmn,skhm,skmhp->skhpn/dot_general | solution.py:152
  173.8 11.7 %fusion.11 = f32[2,16,1,64,128]{4,2,3,1,0:T(1,128)} fusion(f32[2,8,16,1,1]{1,3,4,2,0:T(1,128)S(1)} %copy.119, f32[2,8,16,64,128]{4,3,2,1,0:T(8,128)S(1)} %fusion.3), kind=kOutput, calls=%fused_computation.14 | convolution fusion | flops 25165824 | bytes 9438208 | tf_op jit(solution)/shard_map/sjh,sjhpn->shpn/dot_general | solution.py:164
  188.2 75.4 %collective-permute-done.1 = bf16[4096,256]{1,0:T(8,128)(2,1)S(1)} collective-permute-done((bf16[4096,256]{1,0:T(8,128)(2,1)}, bf16[4096,256]{1,0:T(8,128)(2,1)S(1)}, u32[]{:S(2)}, u32[]{:S(2)}) %collective-permute-start.1) | collective-permute-done | bytes 2097184 | tf_op jit(solution)/shard_map/ppermute | solution.py:16
  264.9 5.1 collective-permute-start.2
  270.0 50.9 %collective-permute-done.2 = bf16[4096,256]{1,0:T(8,128)(2,1)S(1)} collective-permute-done((bf16[4096,256]{1,0:T(8,128)(2,1)S(1)}, bf16[4096,256]{1,0:T(8,128)(2,1)S(1)}, u32[]{:S(2)}, u32[]{:S(2)}) %collective-permute-start.2) | collective-permute-done | bytes 2097184 | tf_op jit(solution)/shard_map/ppermute | solution.py:16
  323.2 91.3 %collective-permute-done.3 = bf16[4096,256]{1,0:T(8,128)(2,1)} collective-permute-done((bf16[4096,256]{1,0:T(8,128)(2,1)S(1)}, bf16[4096,256]{1,0:T(8,128)(2,1)}, u32[]{:S(2)}, u32[]{:S(2)}) %collective-permute-start.3) | collective-permute-done | bytes 2097184 | tf_op jit(solution)/shard_map/ppermute | solution.py:16
  417.4 62.3 %collective-permute-done.4 = bf16[4096,256]{1,0:T(8,128)(2,1)} collective-permute-done((bf16[4096,256]{1,0:T(8,128)(2,1)}, bf16[4096,256]{1,0:T(8,128)(2,1)}, u32[]{:S(2)}, u32[]{:S(2)}) %collective-permute-start.4) | collective-permute-done | bytes 2097184 | tf_op jit(solution)/shard_map/ppermute | solution.py:16
  479.7 5.2 collective-permute-start.5
  484.9 6.0 broadcast_in_dim.31
  499.5 40.7 %all-gather = f32[16,1,16]{2,1,0:T(1,128)S(1)} all-gather(f32[2,1,16]{2,1,0:T(1,128)S(1)} %copy-done.18), channel_id=2, replica_groups=mesh['sp'=8,'tp'=4] {'sp'}, dimensions={0}, use_global_device_ids=true | all-gather | bytes 1152 | tf_op jit(solution)/shard_map/all_gather | solution.py:29
  540.2 4.3 collective-permute-start.6
  544.5 9.3 %convolution_convert_fusion.1 = bf16[1024,1024]{1,0:T(8,128)(2,1)} fusion(bf16[1024,2048]{1,0:T(8,128)(2,1)} %bitcast.121, bf16[2048,1024]{1,0:T(8,128)(2,1)} %all-gather.11.cloned.1.call-done), kind=kOutput, calls=%fused_computation.52 | convolution fusion | flops 4296015872 | bytes 10485760 | tf_op jit(solution)/shard_map/dot_general | solution.py:114
  553.8 9.0 %copy.110 = f32[2,8,64,16,64]{2,4,3,1,0:T(8,128)} copy(f32[2,8,64,16,64]{4,3,2,1,0:T(8,128)} %reshape.114) | data formatting | bytes 8388608 | tf_op jit(solution)/shard_map/reshape | solution.py:138
  564.1 17.2 %fusion.30 = f32[2,8,16,64,128]{4,1,3,2,0:T(8,128)} fusion(f32[2,8,16,64,128]{4,3,2,1,0:T(8,128)} %copy-done.2, f32[2,8,16]{1,2,0:T(8,128)S(1)} %copy.104, f32[2,8,16]{1,2,0:T(8,128)S(1)} %copy.103, pred[8,8]{1,0:T(8,128)(4,1)S(1)} %iota_compare_fusion.1), kind=kOutput, calls=%fused_computation.42 | convolution fusion | flops 201330688 | bytes 16779328 | tf_op jit(solution)/shard_map/skjh,sjhpn->skhpn/dot_general | solution.py:162
  581.4 17.8 %fusion.5 = f32[2,8,16,64,64]{4,3,2,1,0:T(8,128)} fusion(f32[2,8,64,16,64]{4,3,2,1,0:T(8,128)S(1)} %bitcast.111, f32[2,8,64,64]{3,2,1,0:T(8,128)S(1)} %fusion.65, f32[2,8,16,64]{3,2,1,0:T(8,128)S(1)} %reduce_window_sum.24, pred[64,64]{1,0:T(8,128)(4,1)S(1)} %iota_compare_fusion), kind=kOutput, calls=%fused_computation.8 | convolution fusion | flops 808452096 | bytes 8720384 | tf_op jit(solution)/shard_map/skhlm,skmhp->sklhp/dot_general | solution.py:149
  599.3 10.5 %while.12 = (s32[]{:T(128)}, f32[2,16,64,128]{3,2,1,0:T(8,128)S(1)}, s32[]{:T(128)}, f32[8,2,16]{2,1,0:T(2,128)S(1)}, f32[8,2,16,64,128]{4,3,2,1,0:T(8,128)}, /*index=5*/s32[]{:T(128)}, s32[]{:T(128)}, s32[]{:T(128)}) while((s32[]{:T(128)}, f32[2,16,64,128]{3,2,1,0:T(8,128)S(1)}, s32[]{:T(128)}, f32[8,2,16]{2,1,0:T(2,128)S(1)}, ...), condition=%wide.region_4.5_spmd, body=%wide.region_3.4_spmd.sunk | while | flops 524293 | bytes 3146239 | solution.py:37
  609.8 9.0 %fusion.38 = f32[2,8,64,16,64]{2,4,3,1,0:T(8,128)} fusion(f32[2,8,64,128,1]{3,2,4,1,0:T(8,128)S(1)} %bitcast.115, f32[2,16,64,128]{3,2,1,0:T(8,128)S(1)} %get-tuple-element.49), kind=kOutput, calls=%fused_computation.57 | convolution fusion | flops 1610612736 | bytes 5767168 | tf_op jit(solution)/shard_map/skln,shpn,skhl->sklhp/dot_general | solution.py:172
  618.8 18.8 %fusion = f32[2,8,64,16,64]{2,4,3,1,0:T(8,128)} fusion(f32[2,8,16,64,64]{4,3,2,1,0:T(8,128)} %fusion.5, f32[2,8,64,16,64]{2,4,3,1,0:T(8,128)} %copy.110, f32[2,8,64,16,64]{2,4,3,1,0:T(8,128)} %fusion.38, f32[16]{0:T(128)S(1)} %dynamic_slice.37, f32[2,8,64,16]{2,3,1,0:T(8,128)S(1)} %copy-done.10, f32[2,8,64,16]{2,3,1,0:T(8,128)S(1)} %get-tuple-element.62, ...), kind=kOutput, calls=%fused_computation.3 | convolution fusion | flops 1616904192 | bytes 25821248 | tf_op jit(solution)/shard_map/skln,skhpn,skhl->sklhp/dot_general | solution.py:169
  637.5 9.2 %copy.111 = f32[2,8,64,16,64]{4,3,2,1,0:T(8,128)} copy(f32[2,8,64,16,64]{2,4,3,1,0:T(8,128)} %fusion) | data formatting | bytes 8388608 | tf_op jit(solution)/shard_map/add | solution.py:180
  646.7 8.0 %reshape.117 = f32[2,512,1024]{2,1,0:T(8,128)} reshape(f32[2,8,64,16,64]{4,3,2,1,0:T(8,128)} %copy.111) | data formatting | bytes 8388608 | tf_op jit(solution)/shard_map/reshape | solution.py:180
  661.7 3.6 all-to-all-start
  677.8 13.2 %all-to-all-done = bf16[2,512,1024]{2,0,1:T(2,128)(2,1)S(1)} async-done(((bf16[2,512,1024]{2,0,1:T(2,128)(2,1)}), bf16[2,512,1024]{2,0,1:T(2,128)(2,1)S(1)}, u32[]{:S(2)}, u32[]{:S(2)}) %all-to-all-start) | async-done | bytes 2097184 | tf_op jit(solution)/shard_map/all_to_all | solution.py:184
  692.6 5.8 copy.123
  700.7 12.6 %convolution_convert_fusion = bf16[256,2048]{1,0:T(8,128)(2,1)} fusion(bf16[4096,2048]{1,0:T(8,128)(2,1)} %constant_dynamic-update-slice_fusion, f32[256,4096]{1,0:T(8,128)} %bitcast.124, f32[4096]{0:T(1024)S(1)} %copy-done.23, f32[256]{0:T(256)S(1)} %bitcast.141), kind=kOutput, calls=%fused_computation.45 | convolution fusion | flops 4298637312 | bytes 22037504 | tf_op jit(solution)/shard_map/dot_general | solution.py:187
  (149 shorter events, 82.0 us)
Async XLA Ops:
  6.5 74.1 %copy-start = (bf16[2048,64]{0,1:T(8,128)(2,1)S(1)}, bf16[2048,64]{0,1:T(8,128)(2,1)}, u32[]{:S(2)}) copy-start(bf16[2048,64]{0,1:T(8,128)(2,1)} %param.23) | copy-start | bytes 786436
  6.5 5.9 copy-start.15
  6.5 37.4 %copy-start.16 = (bf16[256,128]{1,0:T(8,128)(2,1)S(1)}, bf16[256,128]{1,0:T(8,128)(2,1)}, u32[]{:S(2)}) copy-start(bf16[256,128]{1,0:T(8,128)(2,1)} %param.22) | copy-start | bytes 196612
  6.5 74.1 %all-gather.7.cloned.1.call-start = ((), (), s32[]{:S(2)}) async-start(), calls=%async_computation.1 | async-start | bytes 5242880 | tf_op jit(solution)/shard_map/all_gather | solution.py:109
  10.7 109.9 %all-gather.9.cloned.1.call-start = ((), (), s32[]{:S(2)}) async-start(), calls=%async_computation.2 | async-start | bytes 4718592 | tf_op jit(solution)/shard_map/all_gather | solution.py:90
  11.5 533.1 %all-gather.11.cloned.1.call-start = ((), (), s32[]{:S(2)}) async-start(), calls=%async_computation.3 | async-start | bytes 4718592 | tf_op jit(solution)/shard_map/all_gather | solution.py:89
  12.2 587.0 %all-gather.13.cloned.1.call-start = ((), (), s32[]{:S(2)}) async-start(), calls=%async_computation.4 | async-start | bytes 9437184 | tf_op jit(solution)/shard_map/all_gather | solution.py:29
  129.2 6.4 collective-permute-start
  141.5 8.1 %copy-start.12 = (bf16[1024,128]{1,0:T(8,128)(2,1)S(1)}, bf16[1024,128]{1,0:T(8,128)(2,1)}, u32[]{:S(2)}) copy-start(bf16[1024,128]{1,0:T(8,128)(2,1)} %copy-done.11) | copy-start | bytes 786436
  141.5 8.1 %copy-start.14 = (bf16[1024,128]{1,0:T(8,128)(2,1)S(1)}, bf16[1024,128]{1,0:T(8,128)(2,1)}, u32[]{:S(2)}) copy-start(bf16[1024,128]{1,0:T(8,128)(2,1)} %copy-done.13) | copy-start | bytes 786436
  141.5 8.2 %copy-start.19 = (f32[128]{0:T(128)S(1)}, f32[128]{0:T(128)}, u32[]{:S(2)}) copy-start(f32[128]{0:T(128)} %get-tuple-element.75) | copy-start | bytes 1540
  141.5 8.2 %copy-start.20 = (f32[128]{0:T(128)S(1)}, f32[128]{0:T(128)}, u32[]{:S(2)}) copy-start(f32[128]{0:T(128)} %get-tuple-element.76) | copy-start | bytes 1540
  141.5 8.2 %copy-start.21 = (f32[128]{0:T(128)S(1)}, f32[128]{0:T(128)}, u32[]{:S(2)}) copy-start(f32[128]{0:T(128)} %get-tuple-element.77) | copy-start | bytes 1540
  141.5 8.2 %copy-start.22 = (f32[128]{0:T(128)S(1)}, f32[128]{0:T(128)}, u32[]{:S(2)}) copy-start(f32[128]{0:T(128)} %get-tuple-element.78) | copy-start | bytes 1540
  173.8 11.7 %copy-start.2 = (f32[2,8,16,64,128]{4,3,2,1,0:T(8,128)}, f32[2,8,16,64,128]{4,3,2,1,0:T(8,128)S(1)}, u32[]{:S(2)}) copy-start(f32[2,8,16,64,128]{4,3,2,1,0:T(8,128)S(1)} %fusion.3) | copy-start | bytes 25165828
  173.8 243.5 %copy-start.26 = (f32[64]{0:T(128)S(1)}, f32[64]{0:T(128)}, u32[]{:S(2)}) copy-start(f32[64]{0:T(128)} %param.29) | copy-start | bytes 772
  173.8 243.5 %copy-start.17 = (f32[4,128]{1,0:T(4,128)S(1)}, f32[4,128]{1,0:T(4,128)}, u32[]{:S(2)}) copy-start(f32[4,128]{1,0:T(4,128)} %get-tuple-element.86) | copy-start | bytes 6148
  185.6 78.0 %collective-permute-start.1 = (bf16[4096,256]{1,0:T(8,128)(2,1)}, bf16[4096,256]{1,0:T(8,128)(2,1)S(1)}, u32[]{:S(2)}, u32[]{:S(2)}) collective-permute-start(bf16[4096,256]{1,0:T(8,128)(2,1)} %param.31), channel_id=1, source_target_pairs={{0,4},{4,8},{8,12},{12,16},{16,20},{20,24},{24,28},{28,0},{1,5},{5... | collective-permute-start | bytes 6291464 | tf_op jit(solution)/shard_map/ppermute | solution.py:16
  264.9 56.0 %collective-permute-start.2 = (bf16[4096,256]{1,0:T(8,128)(2,1)S(1)}, bf16[4096,256]{1,0:T(8,128)(2,1)S(1)}, u32[]{:S(2)}, u32[]{:S(2)}) collective-permute-start(bf16[4096,256]{1,0:T(8,128)(2,1)S(1)} %collective-permute-done.1), channel_id=1, source_target_pairs={{0,4},{4,8},{8,12},{12,16},{16,20},{20,24},{24,28},{28,0},{1,5},{5... | collective-permute-start | bytes 6291464 | tf_op jit(solution)/shard_map/ppermute | solution.py:16
  322.2 92.2 %collective-permute-start.3 = (bf16[4096,256]{1,0:T(8,128)(2,1)S(1)}, bf16[4096,256]{1,0:T(8,128)(2,1)}, u32[]{:S(2)}, u32[]{:S(2)}) collective-permute-start(bf16[4096,256]{1,0:T(8,128)(2,1)S(1)} %collective-permute-done.2), channel_id=1, source_target_pairs={{0,4},{4,8},{8,12},{12,16},{16,20},{20,24},{24,28},{28,0},{1,5},{5... | collective-permute-start | bytes 6291464 | tf_op jit(solution)/shard_map/ppermute | solution.py:16
  414.5 65.2 %collective-permute-start.4 = (bf16[4096,256]{1,0:T(8,128)(2,1)}, bf16[4096,256]{1,0:T(8,128)(2,1)}, u32[]{:S(2)}, u32[]{:S(2)}) collective-permute-start(bf16[4096,256]{1,0:T(8,128)(2,1)} %collective-permute-done.3), channel_id=1, source_target_pairs={{0,4},{4,8},{8,12},{12,16},{16,20},{20,24},{24,28},{28,0},{1,5},{5... | collective-permute-start | bytes 6291464 | tf_op jit(solution)/shard_map/ppermute | solution.py:16
  479.7 60.5 %collective-permute-start.5 = (bf16[4096,256]{1,0:T(8,128)(2,1)}, bf16[4096,256]{1,0:T(8,128)(2,1)}, u32[]{:S(2)}, u32[]{:S(2)}) collective-permute-start(bf16[4096,256]{1,0:T(8,128)(2,1)} %collective-permute-done.4), channel_id=1, source_target_pairs={{0,4},{4,8},{8,12},{12,16},{16,20},{20,24},{24,28},{28,0},{1,5},{5... | collective-permute-start | bytes 6291464 | tf_op jit(solution)/shard_map/ppermute | solution.py:16
  484.9 6.0 copy-start.4
  540.2 58.9 %collective-permute-start.6 = (bf16[4096,256]{1,0:T(8,128)(2,1)}, bf16[4096,256]{1,0:T(8,128)(2,1)}, u32[]{:S(2)}, u32[]{:S(2)}) collective-permute-start(bf16[4096,256]{1,0:T(8,128)(2,1)} %collective-permute-done.5), channel_id=1, source_target_pairs={{0,4},{4,8},{8,12},{12,16},{16,20},{20,24},{24,28},{28,0},{1,5},{5... | collective-permute-start | bytes 6291464 | tf_op jit(solution)/shard_map/ppermute | solution.py:16
  563.2 18.2 %slice-start = ((s8[8388608]{0:T(1024)(128)(4,1)}), s8[4194304]{0:T(1024)(128)(4,1)S(1)}, s32[]{:S(2)}) async-start(s8[8388608]{0:T(1024)(128)(4,1)} %bitcast.110), calls=%async_computation.5 | async-start | bytes 8388608
  564.1 17.3 %slice-start.1 = ((s8[8388608]{0:T(1024)(128)(4,1)}), s8[4194304]{0:T(1024)(128)(4,1)S(1)}, s32[]{:S(2)}) async-start(s8[8388608]{0:T(1024)(128)(4,1)} %bitcast.110), calls=%async_computation.6 | async-start | bytes 8388608
  599.2 75.5 %collective-permute-start.7 = (bf16[4096,256]{1,0:T(8,128)(2,1)}, bf16[4096,256]{1,0:T(8,128)(2,1)}, u32[]{:S(2)}, u32[]{:S(2)}) collective-permute-start(bf16[4096,256]{1,0:T(8,128)(2,1)} %collective-permute-done.6), channel_id=1, source_target_pairs={{0,4},{4,8},{8,12},{12,16},{16,20},{20,24},{24,28},{28,0},{1,5},{5... | collective-permute-start | bytes 6291464 | tf_op jit(solution)/shard_map/ppermute | solution.py:16
  609.8 9.0 %copy-start.10 = (f32[2,8,64,16]{2,3,1,0:T(8,128)S(1)}, f32[2,8,64,16]{2,3,1,0:T(8,128)}, u32[]{:S(2)}) copy-start(f32[2,8,64,16]{2,3,1,0:T(8,128)} %get-tuple-element.64) | copy-start | bytes 196612
  646.7 8.0 %copy-start.9 = (bf16[1024,1024]{1,0:T(8,128)(2,1)S(1)}, bf16[1024,1024]{1,0:T(8,128)(2,1)}, u32[]{:S(2)}) copy-start(bf16[1024,1024]{1,0:T(8,128)(2,1)} %convolution_convert_fusion.1) | copy-start | bytes 6291460
  661.7 29.2 %all-to-all-start = ((bf16[2,512,1024]{2,0,1:T(2,128)(2,1)}), bf16[2,512,1024]{2,0,1:T(2,128)(2,1)S(1)}, u32[]{:S(2)}, u32[]{:S(2)}) async-start(bf16[2,512,1024]{2,0,1:T(2,128)(2,1)} %copy.112), calls=%async_computation | async-start | bytes 4194304 | tf_op jit(solution)/shard_map/all_to_all | solution.py:184
  692.6 8.1 %copy-start.23 = (f32[4096]{0:T(1024)S(1)}, f32[4096]{0:T(1024)}, u32[]{:S(2)}) copy-start(f32[4096]{0:T(1024)} %param.30) | copy-start | bytes 49156
  700.7 12.6 %copy-start.1 = (bf16[2048,64]{0,1:T(8,128)(2,1)S(1)}, bf16[2048,64]{0,1:T(8,128)(2,1)}, u32[]{:S(2)}) copy-start(bf16[2048,64]{0,1:T(8,128)(2,1)} %param.23) | copy-start | bytes 786436
  (10 other events, 32.1 us)
Sparse Core Ops, SparseCore 0:
  10.8 35.3 all-gather.6
  48.4 72.1 all-gather.8
  122.7 76.7 all-gather.10
  201.5 257.7 all-gather.12
